TPU v7x, 32 devices: a whole 2x2x4 slice. The times are simulated.
32 devices in a mesh: grp: 2 (over y), sp: 4 (over z), tp: 4 (over x, core).
Axes of the slice: x: 2, y: 2, z: 4, core: 2. Of those that a mesh axis runs over, the one named last changes fastest.
Arguments:
- stream_in: bfloat16 [4096, 2048], P(('grp', 'sp')), parts along dimension 0, may hold values from -6 to 6
- query_wide: bfloat16 [4096, 1024], P(('grp', 'sp'), 'tp'), parts along dimension 0, may hold values from -6 to 6
- key_wide: bfloat16 [4096, 1024], P(('grp', 'sp'), 'tp'), parts along dimension 0, may hold values from -6 to 6
- value_wide: bfloat16 [4096, 2048], P(('grp', 'sp'), 'tp'), parts along dimension 0, may hold values from -6 to 6
- query_narrow: bfloat16 [4096, 512], P(('grp', 'sp'), 'tp'), parts along dimension 0, may hold values from -6 to 6
- key_narrow: bfloat16 [4096, 512], P(('grp', 'sp'), 'tp'), parts along dimension 0, may hold values from -6 to 6
- value_narrow: bfloat16 [4096, 1024], P(('grp', 'sp'), 'tp'), parts along dimension 0, may hold values from -6 to 6
- decay_wide: float32 [4, 4096], P('tp', ('grp', 'sp')), parts along dimension 1, may hold values from -1 to 0
- decay_narrow: float32 [4, 4096], P('tp', ('grp', 'sp')), parts along dimension 1, may hold values from -1 to 0
- gain_wide: float32 [2048], P('tp'), may hold values from 0.1 to 1.9
- gain_narrow: float32 [1024], P('tp'), may hold values from 0.1 to 1.9
- out_wide: bfloat16 [2048, 2048], P('tp'), may hold values from -0.109375 to 0.109375
- out_narrow: bfloat16 [1024, 2048], P('tp'), may hold values from -0.109375 to 0.109375
- mlp_gain: float32 [2048], replicated, may hold values from 0.1 to 1.9
- up_weight: bfloat16 [2048, 8192], P('sp', 'tp'), may hold values from -0.125 to 0.125
- down_weight: bfloat16 [8192, 2048], P('tp', 'sp'), may hold values from -0.0625 to 0.0625
Outputs:
- stream_out: bfloat16 [4096, 2048], P(('grp', 'sp', 'tp')), parts along dimension 0
There are 2 independent parts, one for each index of `grp`. A program takes and returns all parts, laid end to end along the dimension named above; an argument that names none is the same for every part. Nothing has to cross between parts.
All inputs are finite; a program needn't handle non-finite values.
Results may differ from a plain program's by a relative error of at most 0.019.
Values may be sent and summed in bfloat16 or wider, within the bound.
A program may use at most 128 MiB of HBM per device.

v0:
```python
import jax
import jax.numpy as jnp
from jax import lax
from jax.sharding import PartitionSpec as P

EPS = 1e-06


def prefix(x, axis, combine, identity):
    length, mine = (lax.axis_size(axis), lax.axis_index(axis))
    everything = jax.tree.map(
        lambda part, kind: lax.all_gather(part.astype(kind), axis),
        x,
        (jnp.bfloat16, jnp.bfloat16, jnp.bfloat16, jnp.bfloat16),
    )
    start = jax.tree.map(
        lambda part, zero: jnp.broadcast_to(jnp.asarray(zero, part.dtype), part.shape), x, identity
    )

    def step(k, before):
        reached = k < mine
        new = combine(
            before, jax.tree.map(lambda part, own: part[k].astype(own.dtype), everything, x)
        )
        return jax.tree.map(lambda a, b: jnp.where(reached, a, b), new, before)

    return lax.fori_loop(0, length, step, start)


def retain_local(queries, key_rows, value_rows, log_decay):
    total_heads = log_decay.shape[0]
    length = queries.shape[0]
    key_width = queries.shape[1] // total_heads
    value_width = value_rows.shape[1] // total_heads
    query_heads = queries.reshape(length, total_heads, key_width)
    key_heads = key_rows.reshape(length, total_heads, key_width)
    value_heads = value_rows.reshape(length, total_heads, value_width)
    cumulative = jnp.cumsum(log_decay, axis=1)
    row_index = lax.broadcasted_iota(jnp.int32, (length, length), 0)
    col_index = lax.broadcasted_iota(jnp.int32, (length, length), 1)
    causal = (row_index >= col_index)[None]
    log_gap = cumulative[:, :, None] - cumulative[:, None, :]
    fading = jnp.where(causal, jnp.exp(jnp.where(causal, log_gap, 0.0)), 0.0)
    scores = jnp.einsum("ihd,jhd->hij", query_heads, key_heads, preferred_element_type=jnp.float32)
    weights_low = (scores * key_width ** (-0.5) * fading).astype(jnp.bfloat16)
    within = jnp.einsum(
        "hij,jhe->ihe", weights_low, value_heads, preferred_element_type=jnp.float32
    )
    to_end = jnp.exp(cumulative[:, -1:] - cumulative)
    keyed = (key_heads.astype(jnp.float32) * key_width ** (-0.5) * to_end.T[:, :, None]).astype(
        jnp.bfloat16
    )
    local_state = jnp.einsum("jhd,jhe->hde", keyed, value_heads, preferred_element_type=jnp.float32)
    overall = jnp.exp(cumulative[:, -1])
    return (query_heads, cumulative, within, overall, local_state)


def finish(query_heads, cumulative, within, incoming, gain_values):
    carried = (
        jnp.einsum(
            "ihd,hde->ihe",
            query_heads.astype(jnp.float32),
            incoming,
            precision=lax.Precision.HIGHEST,
        )
        * jnp.exp(cumulative).T[:, :, None]
    )
    retained = within + carried
    centered = retained - jnp.mean(retained, axis=-1, keepdims=True)
    scaled = centered * lax.rsqrt(jnp.mean(centered * centered, axis=-1, keepdims=True) + EPS)
    return (scaled.reshape(retained.shape[0], -1) * gain_values).astype(jnp.bfloat16)


def normalize(rows, gain_values):
    values = rows.astype(jnp.float32)
    scaled = values * lax.rsqrt(jnp.mean(values * values, axis=-1, keepdims=True) + EPS)
    return (scaled * gain_values).astype(jnp.bfloat16)


def join_states(earlier, latter):
    return (
        earlier[0] * latter[0],
        latter[0][:, None, None] * earlier[1] + latter[1],
        earlier[2] * latter[2],
        latter[2][:, None, None] * earlier[3] + latter[3],
    )


def on_device(
    stream_in,
    query_wide,
    key_wide,
    value_wide,
    query_narrow,
    key_narrow,
    value_narrow,
    decay_wide,
    decay_narrow,
    gain_wide,
    gain_narrow,
    out_wide,
    out_narrow,
    mlp_gain,
    up_weight,
    down_weight,
):
    length = stream_in.shape[0]
    portion = length // lax.axis_size("tp")
    member = lax.axis_index("tp")
    wide_query, wide_cum, wide_within, wide_factor, wide_state = retain_local(
        query_wide, key_wide, value_wide, decay_wide
    )
    thin_query, thin_cum, thin_within, thin_factor, thin_state = retain_local(
        query_narrow, key_narrow, value_narrow, decay_narrow
    )
    identity = (
        jnp.ones_like(wide_factor),
        jnp.zeros_like(wide_state),
        jnp.ones_like(thin_factor),
        jnp.zeros_like(thin_state),
    )
    incoming = prefix(
        (wide_factor, wide_state, thin_factor, thin_state), "sp", join_states, identity
    )
    normed_wide = finish(wide_query, wide_cum, wide_within, incoming[1], gain_wide)
    normed_thin = finish(thin_query, thin_cum, thin_within, incoming[3], gain_narrow)
    up_full, down_full = (
        lax.all_gather(up_weight, "sp", axis=0, tiled=True),
        lax.all_gather(down_weight, "sp", axis=1, tiled=True),
    )
    mixed_heads = lax.psum(
        (
            jnp.dot(normed_wide, out_wide, preferred_element_type=jnp.float32)
            + jnp.dot(normed_thin, out_narrow, preferred_element_type=jnp.float32)
        ).astype(jnp.bfloat16),
        "tp",
    ).astype(jnp.float32)
    whole_rows = (stream_in.astype(jnp.float32) + mixed_heads).astype(jnp.bfloat16)
    raised = jax.nn.relu(
        jnp.dot(normalize(whole_rows, mlp_gain), up_full, preferred_element_type=jnp.float32)
    )
    hidden = (raised * raised).astype(jnp.bfloat16)
    middle = lax.dynamic_slice_in_dim(whole_rows, member * portion, portion, 0)
    channel = lax.psum_scatter(
        jnp.dot(hidden, down_full, preferred_element_type=jnp.float32).astype(jnp.bfloat16),
        "tp",
        scatter_dimension=0,
        tiled=True,
    ).astype(jnp.float32)
    return (middle.astype(jnp.float32) + channel).astype(jnp.bfloat16)


def solution(mesh):
    placed = (
        P(("grp", "sp"), None),
        P(("grp", "sp"), "tp"),
        P(("grp", "sp"), "tp"),
        P(("grp", "sp"), "tp"),
        P(("grp", "sp"), "tp"),
        P(("grp", "sp"), "tp"),
        P(("grp", "sp"), "tp"),
        P("tp", ("grp", "sp")),
        P("tp", ("grp", "sp")),
        P("tp"),
        P("tp"),
        P("tp", None),
        P("tp", None),
        P(),
        P("sp", "tp"),
        P("tp", "sp"),
    )
    return jax.shard_map(
        on_device,
        mesh=mesh,
        in_specs=placed,
        out_specs=P(("grp", "sp", "tp"), None),
        check_vma=False,
    )
```

profile of v0, /device:TPU:0, one launch (start us, length us, event | category | flops | bytes accessed | tf_op | source)
XLA Modules:
  0.0 481.8 jit_solution(3034267746610162179)
XLA Ops:
  6.5 0.0 copy-start
  6.5 0.0 all-gather.10.cloned.1.call-start
  6.5 1.1 reduce-window.14
  7.7 0.2 slice_reduce_fusion.1
  7.9 0.2 reduce-window.15
  8.0 0.7 fusion.53
  8.7 0.1 broadcast.135
  8.8 0.6 slice.27
  9.4 0.6 slice.26
  11.2 2.3 convolution_convert_fusion.1
  13.4 0.0 all-gather.10.cloned.1.call-update
  13.5 0.0 all-reduce.5.cloned.1.call-start
  13.6 1.0 reduce-window.16
  14.6 0.2 slice_reduce_fusion
  14.7 0.2 reduce-window.19
  14.9 0.1 broadcast.136
  15.0 0.6 slice.29
  15.6 0.6 slice.28
  17.5 1.2 dynamic-slice
  18.7 0.7 dynamic-update-slice
  19.4 0.7 dynamic-update-slice.1
  20.1 14.0 %all-reduce.2 = (bf16[4]{0:T(256)(128)(2,1)S(1)}, bf16[4]{0:T(256)(128)(2,1)S(1)}) all-reduce(bf16[4]{0:T(256)(128)(2,1)S(1)} %dynamic-update-slice, bf16[4]{0:T(256)(128)(2,1)S(1)} %dynamic-update-slice.1), channel_id=1, replica_groups=mesh['grp'=2,'sp'=4,'tp'=4] {'sp'}, use_global_device_ids=true, to_apply=%add | all-reduce | flops 8 | bytes 32
  34.1 0.1 exponential_multiply_fusion
  34.1 1.4 convolution_convert_fusion.2
  35.5 15.4 %all-gather.1 = bf16[512,256]{1,0:T(8,128)(2,1)S(1)} all-gather(bf16[128,256]{1,0:T(8,128)(2,1)S(1)} %convolution_convert_fusion.2), channel_id=3, replica_groups=mesh['grp'=2,'sp'=4,'tp'=4] {'sp'}, dimensions={0}, use_global_device_ids=true | all-gather | bytes 327680 | tf_op jit(solution)/shard_map/all_gather | solution.py:12
  50.9 1.6 fusion.15
  52.6 3.0 convolution_bitcast_fusion.1
  55.6 13.0 %while.16 = (s32[]{:T(128)}, f32[1,256,512]{2,1,0:T(8,128)S(1)}, f32[1,128,256]{2,1,0:T(8,128)S(1)}, s32[]{:T(128)}, bf16[4,1]{0,1:T(2,128)(2,1)S(1)}, /*index=5...) while((s32[]{:T(128)}, f32[1,256,512]{2,1,0:T(8,128)S(1)}, ...), condition=%wide.region_5.6_spmd.clone, body=%wide.region_4.5_spmd.clone.sunk | while | flops 819206 | bytes 1638563 | solution.py:27
  55.6 0.6 constant_dynamic-slice_fusion.3
  56.8 1.3 fusion.81
  58.8 0.1 fusion.82
  58.8 0.6 constant_dynamic-slice_fusion.3
  60.1 1.3 fusion.81
  62.0 0.1 fusion.82
  62.1 0.6 constant_dynamic-slice_fusion.3
  63.3 1.3 fusion.81
  65.3 0.1 fusion.82
  65.3 0.6 constant_dynamic-slice_fusion.3
  66.6 1.3 fusion.81
  68.5 0.1 fusion.82
  68.6 0.0 copy-start.1
  68.6 0.0 copy-start.4
  68.6 0.0 copy-done.3
  68.6 2.5 fusion.55
  71.1 0.2 multiply_reduce_fusion
  71.3 1.4 fusion.54
  72.7 0.1 multiply_reduce_fusion.1
  72.8 0.8 fusion.41
  73.6 2.8 add_convert_fusion.1
  76.5 0.0 all-reduce.5.cloned.1.call-update
  76.5 0.0 all-gather.6.cloned.1.call-start
  76.6 0.7 all-gather.6.cloned.1.call-update
  77.3 0.0 copy-start.6
  77.3 0.0 all-gather.8.cloned.1.call-start
  77.3 0.5 all-gather.8.cloned.1.call-update
  77.8 0.2 reduce-scatter.2.cloned.1.call-start
  78.1 48.4 %all-reduce.5.cloned.1.call-done = bf16[512,2048]{1,0:T(8,128)(2,1)} async-done(((bf16[512,2048]{1,0:T(8,128)(2,1)}), bf16[512,2048]{1,0:T(8,128)(2,1)}) %all-reduce.5.cloned.1.call-update) | async-done | bytes 2097168 | tf_op jit(solution)/shard_map/psum | solution.py:131
  126.5 4.5 fusion.2
  131.1 146.7 %all-gather.6.cloned.1.call-done = bf16[2048,2048]{1,0:T(8,128)(2,1)} async-done(((bf16[512,2048]{1,0:T(8,128)(2,1)}), bf16[2048,2048]{1,0:T(8,128)(2,1)}) %all-gather.6.cloned.1.call-update) | async-done | bytes 8388624 | tf_op jit(solution)/shard_map/all_gather | solution.py:128
  277.8 149.3 %all-gather.8.cloned.1.call-done = bf16[2048,2048]{1,0:T(8,128)(2,1)} async-done(((bf16[2048,512]{1,0:T(8,128)(2,1)}), bf16[2048,2048]{1,0:T(8,128)(2,1)}) %all-gather.8.cloned.1.call-update) | async-done | bytes 8388624 | tf_op jit(solution)/shard_map/all_gather | solution.py:129
  427.1 16.5 %convolution_convert_fusion = bf16[512,2048]{1,0:T(8,128)(2,1)} fusion(bf16[2048,2048]{1,0:T(8,128)(2,1)} %all-gather.8.cloned.1.call-done, bf16[2048,2048]{1,0:T(8,128)(2,1)} %all-gather.6.cloned.1.call-done, bf16[512,2048]{1,0:T(8,128)(2,1)} %get-tuple-element.209, f32[2048]{0:T(1024)S(1)} %copy-done.6, f32[512]{0:T(512)S(1)} %add_rsqrt_fusion), kind=kOutput, calls=%fused_computation.14 | convolution fusion | flops 8598323200 | bytes 20981760 | tf_op jit(solution)/shard_map/dot_general | solution.py:145
  443.6 0.0 reduce-scatter.2.cloned.1.call-update
  443.6 29.5 %reduce-scatter.2.cloned.1.call-done = bf16[128,2048]{1,0:T(8,128)(2,1)} async-done(((bf16[512,2048]{1,0:T(8,128)(2,1)}), bf16[128,2048]{1,0:T(8,128)(2,1)}) %reduce-scatter.2.cloned.1.call-update) | async-done | bytes 524304 | tf_op jit(solution)/shard_map/reduce_scatter | solution.py:144
  473.1 2.1 add_convert_fusion.2
  (23 shorter events, 0.1 us)
Async XLA Ops:
  6.5 67.1 %copy-start = (bf16[512,2048]{1,0:T(8,128)(2,1)S(1)}, bf16[512,2048]{1,0:T(8,128)(2,1)}, u32[]{:S(2)}) copy-start(bf16[512,2048]{1,0:T(8,128)(2,1)} %param.29) | copy-start | bytes 6291460
  6.5 49.1 %all-gather.10.cloned.1.call-start = ((), (), s32[]{:S(2)}) async-start(), calls=%async_computation.5 | async-start | bytes 1310720 | tf_op jit(solution)/shard_map/all_gather | solution.py:12
  8.7 2.4 copy-start.2
  13.5 113.0 %all-reduce.5.cloned.1.call-start = ((), (), s32[]{:S(2)}) async-start(), calls=%async_computation.1 | async-start | bytes 4194304 | tf_op jit(solution)/shard_map/psum | solution.py:131
  55.6 13.0 %copy-start.3 = (f32[512]{0:T(512)S(1)}, f32[512]{0:T(512)}, u32[]{:S(2)}) copy-start(f32[512]{0:T(512)} %get-tuple-element.210) | copy-start | bytes 6148
  68.6 4.2 copy-start.1
  68.6 4.2 copy-start.4
  72.8 0.9 copy-start.5
  76.5 201.3 %all-gather.6.cloned.1.call-start = ((), (), s32[]{:S(2)}) async-start(), calls=%async_computation.2 | async-start | bytes 10485760 | tf_op jit(solution)/shard_map/all_gather | solution.py:128
  77.3 349.8 %copy-start.6 = (f32[2048]{0:T(1024)S(1)}, f32[2048]{0:T(1024)}, u32[]{:S(2)}) copy-start(f32[2048]{0:T(1024)} %param.31) | copy-start | bytes 24580
  77.3 349.8 %all-gather.8.cloned.1.call-start = ((), (), s32[]{:S(2)}) async-start(), calls=%async_computation.3 | async-start | bytes 10485760 | tf_op jit(solution)/shard_map/all_gather | solution.py:129
  77.8 395.3 %reduce-scatter.2.cloned.1.call-start = ((), (), s32[]{:S(2)}) async-start(), calls=%async_computation.4 | async-start | bytes 2621440 | tf_op jit(solution)/shard_map/reduce_scatter | solution.py:144
Sparse Core Ops, SparseCore 0:
  13.6 34.9 all-gather.9
  76.6 49.8 all-reduce.4
  128.1 149.6 all-gather.5
  279.2 147.7 all-gather.7
  443.7 29.3 reduce-scatter.1
where the time goes:
time: 482 us
  waiting for transfers between devices  375 us (78%)
  matrix products  32.3 us (7%)
  blocking collectives  29.4 us (6%)
  between operations  15.8 us (3%)
  other arithmetic  15.5 us (3%)
  local copies, waits for them, and re-layouts  8.03 us (2%)
  loops' own time  5.17 us (1%)
    all_gather x1, waiting for transfers between devices, on_device(): lax.all_gather(down_weight, 'sp', axis=1, tiled=True)  149 us
    all_gather x1, waiting for transfers between devices, on_device(): lax.all_gather(up_weight, 'sp', axis=0, tiled=True)  147 us
    psum x1, waiting for transfers between devices, on_device(): lax.psum((jnp.dot(normed_wide, out_wide, preferred_element_type=jnp.float...  48.4 us
    reduce_scatter x1, waiting for transfers between devices, on_device(): lax.psum_scatter(jnp.dot(hidden, down_full, preferred_element_type=jnp.fl...  29.5 us
    dot_general x1, matrix products, on_device(): jnp.dot(hidden, down_full, preferred_element_type=jnp.float32)  16.5 us
    all_gather x1, blocking collectives, prefix(): lax.all_gather(part.astype(kind), axis)  15.4 us
    unnamed x1, blocking collectives  14 us
  transfers between devices with their start and end apart: 5, of which 4 were waited for; matrix products, arithmetic and copies ran while one was open for 3% of the time, Pallas kernels for 0%

commit v1 on v0

--- a/solution.py
+++ b/solution.py
@@ -128,12 +128,15 @@
         lax.all_gather(up_weight, "sp", axis=0, tiled=True),
         lax.all_gather(down_weight, "sp", axis=1, tiled=True),
     )
-    mixed_heads = lax.psum(
-        (
-            jnp.dot(normed_wide, out_wide, preferred_element_type=jnp.float32)
-            + jnp.dot(normed_thin, out_narrow, preferred_element_type=jnp.float32)
-        ).astype(jnp.bfloat16),
-        "tp",
+    mixed_heads = jnp.sum(
+        lax.all_gather(
+            (
+                jnp.dot(normed_wide, out_wide, preferred_element_type=jnp.float32)
+                + jnp.dot(normed_thin, out_narrow, preferred_element_type=jnp.float32)
+            ).astype(jnp.bfloat16),
+            "tp",
+        ),
+        axis=0,
     ).astype(jnp.float32)
     whole_rows = (stream_in.astype(jnp.float32) + mixed_heads).astype(jnp.bfloat16)
     raised = jax.nn.relu(

time: 482 us -> 489 us (1.015)
  other arithmetic: 15.5 us -> 23.4 us
    all_gather x0 -> x1, waiting for transfers between devices: none -> 55.3 us  [on_device(): lax.all_gather((jnp.dot(normed_wide, out_wide, preferred_element_type=jnp...]
    psum x1 -> x0, waiting for transfers between devices: 48.4 us -> none  [on_device(): lax.psum((jnp.dot(normed_wide, out_wide, preferred_element_type=jnp.float...]
    all_gather x1, waiting for transfers between devices: 149 us -> 139 us  [on_device(): lax.all_gather(down_weight, 'sp', axis=1, tiled=True)]
    reduce_sum x0 -> x1, other arithmetic: none -> 7.27 us  [on_device(): jnp.sum(lax.all_gather((jnp.dot(normed_wide, out_wide, preferred_element_...]
  transfers between devices with their start and end apart: 5 -> 5, of which waited for: 4 -> 4; matrix products, arithmetic and copies ran while one was open for 3% -> 5% of each run, Pallas kernels for 0% -> 0%
where the time goes in v1:
time: 489 us
  waiting for transfers between devices  374 us (76%)
  matrix products  32.4 us (7%)
  blocking collectives  29.4 us (6%)
  other arithmetic  23.4 us (5%)
  between operations  15.8 us (3%)
  local copies, waits for them, and re-layouts  8.03 us (2%)
  loops' own time  5.16 us (1%)
    all_gather x1, waiting for transfers between devices, on_device(): lax.all_gather(up_weight, 'sp', axis=0, tiled=True)  149 us
    all_gather x1, waiting for transfers between devices, on_device(): lax.all_gather(down_weight, 'sp', axis=1, tiled=True)  139 us
    all_gather x1, waiting for transfers between devices, on_device(): lax.all_gather((jnp.dot(normed_wide, out_wide, preferred_element_type=jnp...  55.3 us
    reduce_scatter x1, waiting for transfers between devices, on_device(): lax.psum_scatter(jnp.dot(hidden, down_full, preferred_element_type=jnp.fl...  29.5 us
    dot_general x1, matrix products, on_device(): jnp.dot(hidden, down_full, preferred_element_type=jnp.float32)  16.6 us
    all_gather x1, blocking collectives, prefix(): lax.all_gather(part.astype(kind), axis)  15.4 us
    unnamed x1, blocking collectives  14 us
  transfers between devices with their start and end apart: 5, of which 4 were waited for; matrix products, arithmetic and copies ran while one was open for 5% of the time, Pallas kernels for 0%

profile of v1, /device:TPU:0, one launch (start us, length us, event | category | flops | bytes accessed | tf_op | source)
XLA Modules:
  0.0 488.7 jit_solution(3423841543137919722)
XLA Ops:
  6.5 0.0 all-gather.12.cloned.1.call-start
  6.5 1.1 reduce-window.14
  7.7 0.2 slice_reduce_fusion.1
  7.9 0.2 reduce-window.15
  8.0 0.7 fusion.53
  8.7 0.1 broadcast.135
  8.8 0.6 slice.27
  9.4 0.6 slice.26
  11.2 2.3 convolution_convert_fusion.1
  13.4 0.0 all-gather.12.cloned.1.call-update
  13.5 0.0 all-gather.14.cloned.1.call-start
  13.6 1.0 reduce-window.16
  14.6 0.2 slice_reduce_fusion
  14.7 0.2 reduce-window.19
  14.9 0.1 broadcast.136
  15.0 0.6 slice.29
  15.6 0.6 slice.28
  17.5 1.2 dynamic-slice
  18.7 0.7 dynamic-update-slice
  19.4 0.7 dynamic-update-slice.1
  20.1 14.0 %all-reduce.2 = (bf16[4]{0:T(256)(128)(2,1)S(1)}, bf16[4]{0:T(256)(128)(2,1)S(1)}) all-reduce(bf16[4]{0:T(256)(128)(2,1)S(1)} %dynamic-update-slice, bf16[4]{0:T(256)(128)(2,1)S(1)} %dynamic-update-slice.1), channel_id=1, replica_groups=mesh['grp'=2,'sp'=4,'tp'=4] {'sp'}, use_global_device_ids=true, to_apply=%add | all-reduce | flops 8 | bytes 32
  34.1 0.1 exponential_multiply_fusion
  34.1 1.4 convolution_convert_fusion.2
  35.5 15.4 %all-gather.1 = bf16[512,256]{1,0:T(8,128)(2,1)S(1)} all-gather(bf16[128,256]{1,0:T(8,128)(2,1)S(1)} %convolution_convert_fusion.2), channel_id=3, replica_groups=mesh['grp'=2,'sp'=4,'tp'=4] {'sp'}, dimensions={0}, use_global_device_ids=true | all-gather | bytes 327680 | tf_op jit(solution)/shard_map/all_gather | solution.py:12
  50.9 1.6 fusion.15
  52.6 3.0 convolution_bitcast_fusion.1
  55.6 13.0 %while.16 = (s32[]{:T(128)}, f32[1,256,512]{2,1,0:T(8,128)S(1)}, f32[1,128,256]{2,1,0:T(8,128)S(1)}, s32[]{:T(128)}, bf16[4,1]{0,1:T(2,128)(2,1)S(1)}, /*index=5...) while((s32[]{:T(128)}, f32[1,256,512]{2,1,0:T(8,128)S(1)}, ...), condition=%wide.region_5.6_spmd.clone, body=%wide.region_4.5_spmd.clone.sunk | while | flops 819206 | bytes 1638563 | solution.py:27
  55.6 0.6 constant_dynamic-slice_fusion.3
  56.8 1.3 fusion.81
  58.8 0.1 fusion.82
  58.8 0.6 constant_dynamic-slice_fusion.3
  60.1 1.3 fusion.81
  62.0 0.1 fusion.82
  62.1 0.6 constant_dynamic-slice_fusion.3
  63.3 1.3 fusion.81
  65.3 0.1 fusion.82
  65.3 0.6 constant_dynamic-slice_fusion.3
  66.6 1.3 fusion.81
  68.5 0.1 fusion.82
  68.6 0.0 copy-start.1
  68.6 0.0 copy-start.4
  68.6 0.0 copy-done.3
  68.6 2.5 fusion.55
  71.1 0.2 multiply_reduce_fusion
  71.3 1.4 fusion.54
  72.7 0.1 multiply_reduce_fusion.1
  72.8 0.8 fusion.41
  73.7 2.9 add_convert_fusion.1
  76.5 0.0 all-gather.14.cloned.1.call-update
  76.6 0.0 all-gather.10.cloned.1.call-start
  76.6 0.7 all-gather.10.cloned.1.call-update
  77.3 0.0 all-gather.8.cloned.1.call-start
  77.3 0.5 all-gather.8.cloned.1.call-update
  77.9 0.2 reduce-scatter.2.cloned.1.call-start
  78.1 55.3 %all-gather.14.cloned.1.call-done = bf16[2048,2048]{1,0:T(8,128)(2,1)} async-done(((bf16[512,2048]{1,0:T(8,128)(2,1)}), bf16[2048,2048]{1,0:T(8,128)(2,1)}) %all-gather.14.cloned.1.call-update) | async-done | bytes 8388624 | tf_op jit(solution)/shard_map/all_gather | solution.py:132
  133.4 7.3 %reduce_sum.61 = bf16[512,2048]{1,0:T(8,128)(2,1)} reduce(bf16[4,512,2048]{2,1,0:T(8,128)(2,1)} %bitcast.119, bf16[]{:T(256)} %constant.63.clone.1), dimensions={0}, to_apply=%region_10.11 | reduce | flops 3145728 | bytes 10485762 | tf_op jit(solution)/shard_map/reduce_sum | solution.py:131
  140.7 5.1 %fusion.2 = (f32[512]{0:T(512)S(1)}, bf16[512,2048]{1,0:T(8,128)(2,1)}) fusion(bf16[512,2048]{1,0:T(8,128)(2,1)} %reduce_sum.61, bf16[512,2048]{1,0:T(8,128)(2,1)} %param.18), kind=kLoop, calls=%fused_computation.8 | loop fusion | flops 7339520 | bytes 6293504 | tf_op jit(solution)/shard_map/reduce_sum | solution.py:76
  145.9 138.8 %all-gather.10.cloned.1.call-done = bf16[2048,2048]{1,0:T(8,128)(2,1)} async-done(((bf16[2048,512]{1,0:T(8,128)(2,1)}), bf16[2048,2048]{1,0:T(8,128)(2,1)}) %all-gather.10.cloned.1.call-update) | async-done | bytes 8388624 | tf_op jit(solution)/shard_map/all_gather | solution.py:129
  284.7 149.3 %all-gather.8.cloned.1.call-done = bf16[2048,2048]{1,0:T(8,128)(2,1)} async-done(((bf16[512,2048]{1,0:T(8,128)(2,1)}), bf16[2048,2048]{1,0:T(8,128)(2,1)}) %all-gather.8.cloned.1.call-update) | async-done | bytes 8388624 | tf_op jit(solution)/shard_map/all_gather | solution.py:128
  433.9 0.0 copy-done.6
  433.9 16.6 %convolution_convert_fusion = bf16[512,2048]{1,0:T(8,128)(2,1)} fusion(bf16[2048,2048]{1,0:T(8,128)(2,1)} %all-gather.10.cloned.1.call-done, bf16[2048,2048]{1,0:T(8,128)(2,1)} %all-gather.8.cloned.1.call-done, bf16[512,2048]{1,0:T(8,128)(2,1)} %get-tuple-element.209, f32[2048]{0:T(1024)S(1)} %copy-done.6, f32[512]{0:T(512)S(1)} %add_rsqrt_fusion), kind=kOutput, calls=%fused_computation.14 | convolution fusion | flops 8598323200 | bytes 20981760 | tf_op jit(solution)/shard_map/dot_general | solution.py:148
  450.5 0.0 reduce-scatter.2.cloned.1.call-update
  450.5 29.5 %reduce-scatter.2.cloned.1.call-done = bf16[128,2048]{1,0:T(8,128)(2,1)} async-done(((bf16[512,2048]{1,0:T(8,128)(2,1)}), bf16[128,2048]{1,0:T(8,128)(2,1)}) %reduce-scatter.2.cloned.1.call-update) | async-done | bytes 524304 | tf_op jit(solution)/shard_map/reduce_scatter | solution.py:147
  480.1 2.1 add_convert_fusion.2
  (24 shorter events, 0.1 us)
Async XLA Ops:
  6.5 67.1 %copy-start = (bf16[512,2048]{1,0:T(8,128)(2,1)S(1)}, bf16[512,2048]{1,0:T(8,128)(2,1)}, u32[]{:S(2)}) copy-start(bf16[512,2048]{1,0:T(8,128)(2,1)} %param.29) | copy-start | bytes 6291460
  6.5 49.1 %all-gather.12.cloned.1.call-start = ((), (), s32[]{:S(2)}) async-start(), calls=%async_computation.4 | async-start | bytes 1310720 | tf_op jit(solution)/shard_map/all_gather | solution.py:12
  8.7 2.4 copy-start.2
  13.5 120.0 %all-gather.14.cloned.1.call-start = ((), (), s32[]{:S(2)}) async-start(), calls=%async_computation.5 | async-start | bytes 10485760 | tf_op jit(solution)/shard_map/all_gather | solution.py:132
  55.6 13.0 %copy-start.3 = (f32[512]{0:T(512)S(1)}, f32[512]{0:T(512)}, u32[]{:S(2)}) copy-start(f32[512]{0:T(512)} %get-tuple-element.210) | copy-start | bytes 6148
  68.6 4.2 copy-start.1
  68.6 4.2 copy-start.4
  72.8 0.9 copy-start.5
  76.6 208.1 %all-gather.10.cloned.1.call-start = ((), (), s32[]{:S(2)}) async-start(), calls=%async_computation.2 | async-start | bytes 10485760 | tf_op jit(solution)/shard_map/all_gather | solution.py:129
  77.3 356.6 %all-gather.8.cloned.1.call-start = ((), (), s32[]{:S(2)}) async-start(), calls=%async_computation.1 | async-start | bytes 10485760 | tf_op jit(solution)/shard_map/all_gather | solution.py:128
  77.9 402.2 %reduce-scatter.2.cloned.1.call-start = ((), (), s32[]{:S(2)}) async-start(), calls=%async_computation.3 | async-start | bytes 2621440 | tf_op jit(solution)/shard_map/reduce_scatter | solution.py:147
  140.7 293.2 %copy-start.6 = (f32[2048]{0:T(1024)S(1)}, f32[2048]{0:T(1024)}, u32[]{:S(2)}) copy-start(f32[2048]{0:T(1024)} %param.31) | copy-start | bytes 24580
Sparse Core Ops, SparseCore 0:
  13.6 34.9 all-gather.11
  76.7 56.7 all-gather.13
  135.0 149.6 all-gather.9
  286.1 147.7 all-gather.7
  450.7 29.3 reduce-scatter.1
